TPU v7x, 32 devices: a whole 2x2x4 slice. The times are simulated.
32 devices in a mesh: ep: 8 (over z, core), tp: 4 (over y, x).
Axes of the slice: x: 2, y: 2, z: 4, core: 2. Of those that a mesh axis runs over, the one named last changes fastest.
Arguments:
- first_batch_queries: bfloat16 [2048, 1024], P('ep', 'tp'), may hold values from -6 to 6
- first_batch_keys: bfloat16 [2048, 1024], P('ep', 'tp'), may hold values from -6 to 6
- first_batch_values: bfloat16 [2048, 2048], P('ep', 'tp'), may hold values from -6 to 6
- output_gate_preactivation: bfloat16 [2048, 2048], P('ep', 'tp'), may hold values from -6 to 6
- decay_preactivation: bfloat16 [2048, 1024], P('ep', 'tp'), may hold values from -6 to 6
- channel_decay_bias: float32 [1024], P('tp')
- added_log_decay: float32 [16, 2048], P('tp', 'ep'), may hold values from -0.7 to 0
- head_norm_gain: float32 [2048], P('tp'), may hold values from 0.1 to 1.9
- attention_output_weight: bfloat16 [2048, 2048], P(None, 'tp'), may hold values from -0.125 to 0.125
- second_batch_rows: bfloat16 [768, 2048], P('ep'), may hold values from -6 to 6
- expert_norm_gain: float32 [2048], replicated, may hold values from 0.1 to 1.9
- routed_expert_index: int32 [768, 4], P('ep'), may hold values from 0 to 7, all different within a row; in each aligned block of 96 rows (0 to 95, 96 to 191, ...) at most 72 rows name the same one
- router_chosen_scores: float32 [768, 4], P('ep'), may hold values from 0.1 to 1
- expert_gate_weight: bfloat16 [8, 2048, 4096], P('ep', None, 'tp'), may hold values from -0.125 to 0.125
- expert_up_weight: bfloat16 [8, 2048, 4096], P('ep', None, 'tp'), may hold values from -0.125 to 0.125
- expert_down_weight: bfloat16 [8, 4096, 2048], P('ep', None, 'tp'), may hold values from -0.09375 to 0.09375
- shared_gate_weight: bfloat16 [2048, 1024], P(None, 'tp'), may hold values from -0.125 to 0.125
- shared_up_weight: bfloat16 [2048, 1024], P(None, 'tp'), may hold values from -0.125 to 0.125
- shared_down_weight: bfloat16 [1024, 2048], P(None, 'tp'), may hold values from -0.1875 to 0.1875
Outputs:
- token_mixed: bfloat16 [2048, 2048], P('ep', 'tp')
- channel_mixed: bfloat16 [768, 2048], P('ep', 'tp')
Inputs may be any that keep to these rules, and one draw needn't show every extreme that they name: `routed_expert_index`: in each aligned block of 96 rows (the rows of one index of ep) no expert is named by more than 72 rows, a bound that some block reaches; a row names 4 different experts.
All inputs are finite; a program needn't handle non-finite values.
Results may differ from a plain program's by a relative error of at most 0.018.
Values may be sent and summed in bfloat16 or wider, within the bound.
A program may use at most 64 MiB of HBM per device.

v0:
```python
import jax
import jax.numpy as jnp
from jax import lax
from jax.sharding import PartitionSpec as P

BLOCK = 64
epsilon = 1e-06
temper = 16.0
routed_scale = 2.5
largest_value = lax.Precision.HIGHEST


def entering(value, axis, combine, identity):
    size, here = (lax.axis_size(axis), lax.axis_index(axis))
    everything = jax.tree.map(
        lambda part, kind: lax.all_gather(part.astype(kind), axis),
        value,
        (jnp.bfloat16, jnp.bfloat16),
    )
    start = jax.tree.map(
        lambda part, zero: jnp.broadcast_to(jnp.asarray(zero, part.dtype), part.shape),
        value,
        identity,
    )

    def hop(k, before):
        reached = k < here
        new = combine(
            before, jax.tree.map(lambda part, own: part[k].astype(own.dtype), everything, value)
        )
        return jax.tree.map(lambda a, b: jnp.where(reached, a, b), new, before)

    return lax.fori_loop(0, size, hop, start)


def head_norm(tensor, gain_rows):
    mean_square = jnp.mean(tensor * tensor, axis=-1, keepdims=True)
    return tensor * lax.rsqrt(mean_square + epsilon) * gain_rows


def log_decay_values(decay_preactivation, channel_decay_bias, added_log_decay):
    number_of_heads = added_log_decay.shape[0]
    row_count = decay_preactivation.shape[0]
    logits = decay_preactivation.astype(jnp.float32) + channel_decay_bias[None, :]
    baseline_log_decay = (jax.nn.log_sigmoid(logits) / temper).reshape(
        row_count, number_of_heads, -1
    )
    return baseline_log_decay + jnp.transpose(added_log_decay)[:, :, None]


def combine_states(earlier, latter):
    return (earlier[0] * latter[0], latter[0][..., None] * earlier[1] + latter[1])


def mixer_heads(
    first_batch_queries,
    first_batch_keys,
    first_batch_values,
    output_gate_preactivation,
    decay_preactivation,
    channel_decay_bias,
    added_log_decay,
    head_norm_gain,
):
    number_of_heads = added_log_decay.shape[0]
    row_count = first_batch_queries.shape[0]
    key_channel_width = first_batch_queries.shape[1] // number_of_heads
    value_width = first_batch_values.shape[1] // number_of_heads
    block_count = row_count // BLOCK

    def split_into_blocks(tensor, width):
        shaped = tensor.astype(jnp.float32).reshape(block_count, BLOCK, number_of_heads, width)
        return shaped.transpose(0, 2, 1, 3)

    queries = split_into_blocks(first_batch_queries, key_channel_width)
    keys_all = split_into_blocks(first_batch_keys, key_channel_width)
    values = split_into_blocks(first_batch_values, value_width)
    decay_factors = split_into_blocks(
        log_decay_values(decay_preactivation, channel_decay_bias, added_log_decay),
        key_channel_width,
    )
    running_state = jnp.cumsum(decay_factors, axis=2)
    block_number_total = running_state[:, :, -1, :]
    query_decayed = queries * jnp.exp(running_state)
    key_raised = keys_all * jnp.exp(-running_state)
    lower_mask = jnp.tril(jnp.ones((BLOCK, BLOCK), bool))
    attention_scores = jnp.einsum(
        "nhqd,nhkd->nhqk", query_decayed, key_raised, precision=largest_value
    )
    attention_scores = jnp.where(lower_mask, attention_scores, 0.0)
    within_block = jnp.einsum("nhqk,nhkv->nhqv", attention_scores, values, precision=largest_value)
    updates = jnp.einsum(
        "nhkd,nhkv->nhdv",
        keys_all * jnp.exp(block_number_total[:, :, None, :] - running_state),
        values,
        precision=largest_value,
    )

    def carry_blocks(carry_state, inputs):
        state_update, total_log = inputs
        return (jnp.exp(total_log)[..., None] * carry_state + state_update, carry_state)

    zero_state = jnp.zeros((number_of_heads, key_channel_width, value_width), jnp.float32)
    device_state, before = lax.scan(carry_blocks, zero_state, (updates, block_number_total))
    device_decay = jnp.exp(jnp.sum(block_number_total, axis=0))
    identity = (jnp.ones((number_of_heads, key_channel_width), jnp.float32), zero_state)
    _, incoming = entering((device_decay, device_state), "ep", combine_states, identity)
    lead_in = jnp.exp(jnp.cumsum(block_number_total, axis=0) - block_number_total)
    states = before + lead_in[..., None] * incoming[None]
    carried = jnp.einsum("nhqd,nhdv->nhqv", query_decayed, states, precision=largest_value)
    head_values = (
        (within_block + carried)
        .transpose(0, 2, 1, 3)
        .reshape(row_count, number_of_heads, value_width)
    )
    gate_rows = jax.nn.silu(output_gate_preactivation.astype(jnp.float32)).reshape(
        row_count, number_of_heads, value_width
    )
    gated_heads = (
        head_norm(head_values, head_norm_gain.reshape(number_of_heads, value_width)) * gate_rows
    )
    return gated_heads.reshape(row_count, number_of_heads * value_width).astype(jnp.bfloat16)


def expert_slots(route_rows, experts, capacity):
    flat_ids = route_rows.reshape(-1)
    targets = jnp.arange(experts, dtype=jnp.int32)
    onehot = (flat_ids[:, None] == targets[None, :]).astype(jnp.int32)
    earlier = jnp.cumsum(onehot, axis=0) - onehot
    return flat_ids * capacity + jnp.sum(earlier * onehot, axis=1)


def slot_owner(slot_ids, slot_count, top_count):
    matches = slot_ids[None, :] == jnp.arange(slot_count, dtype=jnp.int32)[:, None]
    token_ids = jnp.arange(slot_ids.shape[0], dtype=jnp.int32) // top_count
    return jnp.sum(jnp.where(matches, token_ids[None, :] + 1, 0), axis=1) - 1


def fill_slots(source_rows, owners):
    picked_rows = jnp.take(source_rows, jnp.maximum(owners, 0), axis=0)
    return jnp.where((owners >= 0)[:, None], picked_rows, jnp.zeros((), jnp.bfloat16))


def paired_rows(tensor, factor):
    return tensor.reshape(tensor.shape[0] // factor, tensor.shape[1] * factor)


def paired_product(section, weight, factor, own_width):
    row_count = section.shape[0]
    pieces = section.reshape(row_count, -1, factor, own_width)
    products = [
        jnp.dot(
            pieces[:, :, which, :].reshape(row_count, -1),
            weight,
            preferred_element_type=jnp.float32,
        )
        for which in range(factor)
    ]
    return jnp.stack(products, axis=1)


def local(
    first_batch_queries,
    first_batch_keys,
    first_batch_values,
    output_gate_preactivation,
    decay_preactivation,
    channel_decay_bias,
    added_log_decay,
    head_norm_gain,
    attention_output_weight,
    second_batch_rows,
    expert_norm_gain,
    routed_expert_index,
    router_chosen_scores,
    expert_gate_weight,
    expert_up_weight,
    expert_down_weight,
    shared_gate_weight,
    shared_up_weight,
    shared_down_weight,
):
    mixed_heads = mixer_heads(
        first_batch_queries,
        first_batch_keys,
        first_batch_values,
        output_gate_preactivation,
        decay_preactivation,
        channel_decay_bias,
        added_log_decay,
        head_norm_gain,
    )
    experts = lax.axis_size("ep")
    tokens, top_count = routed_expert_index.shape
    capacity = tokens * top_count * 3 // (2 * experts)
    slot_count = experts * capacity
    model_width = second_batch_rows.shape[1]
    features = second_batch_rows.astype(jnp.float32)
    normed = features * lax.rsqrt(jnp.mean(features * features, axis=1, keepdims=True) + epsilon)
    normed = (normed * expert_norm_gain[None, :]).astype(jnp.bfloat16)
    slot_ids = expert_slots(routed_expert_index, experts, capacity)
    owners = slot_owner(slot_ids, slot_count, top_count)
    gate_weight = expert_gate_weight[0]
    up_weight = expert_up_weight[0]
    down_weight = expert_down_weight[0]
    columns = model_width // lax.axis_size("tp")
    own_columns = lax.dynamic_slice_in_dim(normed, lax.axis_index("tp") * columns, columns, 1)
    outgoing = fill_slots(own_columns, owners).reshape(experts, capacity, columns)
    arrived = lax.all_to_all(outgoing, "ep", split_axis=0, concat_axis=0, tiled=True)
    flat_columns = arrived.reshape(slot_count, columns)
    section = lax.all_gather(flat_columns, "tp", axis=1, tiled=True)
    gate_value = jnp.dot(section, gate_weight, preferred_element_type=jnp.float32)
    up_value = jnp.dot(section, up_weight, preferred_element_type=jnp.float32)
    routed_hidden = (jax.nn.silu(gate_value) * up_value).astype(jnp.bfloat16)
    hidden_width = routed_hidden.shape[1]
    shared_gate_value = jnp.dot(normed, shared_gate_weight, preferred_element_type=jnp.float32)
    shared_up_value = jnp.dot(normed, shared_up_weight, preferred_element_type=jnp.float32)
    shared_hidden = (jax.nn.silu(shared_gate_value) * shared_up_value).astype(jnp.bfloat16)
    shared_width = shared_hidden.shape[1]
    shared_factor = hidden_width // shared_width
    shared_paired = paired_rows(shared_hidden, shared_factor)
    mixer_total = jnp.dot(
        lax.all_gather(mixed_heads, "tp", axis=1, tiled=True),
        attention_output_weight,
        preferred_element_type=jnp.float32,
    )
    routed_section = lax.all_gather(routed_hidden, "tp", axis=1, tiled=True)
    shared_section = lax.all_gather(shared_paired, "tp", axis=1, tiled=True)
    routed_part = jnp.dot(routed_section, down_weight, preferred_element_type=jnp.float32)
    shared_part = paired_product(shared_section, shared_down_weight, shared_factor, shared_width)
    shared_total = shared_part.reshape(tokens, -1)
    token_mixed = mixer_total.astype(jnp.bfloat16)
    routed_output = routed_part.astype(jnp.bfloat16).reshape(experts, capacity, -1)
    returned = lax.all_to_all(routed_output, "ep", split_axis=0, concat_axis=0, tiled=True).reshape(
        slot_count, -1
    )
    picked = jnp.take(returned, slot_ids, axis=0).astype(jnp.float32).reshape(tokens, top_count, -1)
    weights = (
        routed_scale * router_chosen_scores / jnp.sum(router_chosen_scores, axis=1, keepdims=True)
    )
    channel_mixed = (jnp.sum(weights[:, :, None] * picked, axis=1) + shared_total).astype(
        jnp.bfloat16
    )
    return (token_mixed, channel_mixed)


def solution(mesh):
    placed = (
        P("ep", "tp"),
        P("ep", "tp"),
        P("ep", "tp"),
        P("ep", "tp"),
        P("ep", "tp"),
        P("tp"),
        P("tp", "ep"),
        P("tp"),
        P(None, "tp"),
        P("ep", None),
        P(),
        P("ep", None),
        P("ep", None),
        P("ep", None, "tp"),
        P("ep", None, "tp"),
        P("ep", None, "tp"),
        P(None, "tp"),
        P(None, "tp"),
        P(None, "tp"),
    )
    return jax.shard_map(
        local, mesh=mesh, in_specs=placed, out_specs=(P("ep", "tp"), P("ep", "tp")), check_vma=False
    )
```

profile of v0, /device:TPU:0, one launch (start us, length us, event | category | flops | bytes accessed | tf_op | source)
XLA Modules:
  0.0 203.9 jit_solution(17407363473838470241)
XLA Ops:
  13.7 2.7 %gather_fusion = bf16[576,512]{1,0:T(8,128)(2,1)S(1)} fusion(bf16[96,512]{1,0:T(8,128)(2,1)S(1)} %constant_dynamic-slice_fusion, s32[1024]{0:T(1024)S(1)} %pad_clamp_fusion.1), kind=kCustom, calls=%fused_computation | custom fusion | bytes 1181952 | tf_op jit(solution)/shard_map/jit(_take)/gather | solution.py:140
  16.7 23.0 %all_to_all.10 = bf16[8,72,512]{2,1,0:T(8,128)(2,1)} all-to-all(bf16[8,72,512]{2,1,0:T(8,128)(2,1)S(1)} %select_select_fusion), channel_id=1, replica_groups=mesh['ep'=8,'tp'=4] {'ep'}, dimensions={0} | all-to-all | bytes 1179648 | tf_op jit(solution)/shard_map/all_to_all | solution.py:209
  40.6 1.7 reshape.254
  43.4 1.5 reduce_window_sum.37
  44.9 2.4 %fusion.23 = f32[4,4,64,128]{3,2,1,0:T(8,128)} fusion(f32[4,4,64,64]{3,2,1,0:T(8,128)S(1)} %reduce_window_sum.37, f32[4,64,4,64]{3,2,1,0:T(4,128)S(1)} %reshape.267, f32[4,4,64]{2,1,0:T(4,128)S(1)} %bitcast.133, bf16[4,64,4,128]{3,2,1,0:T(4,128)(2,1)} %reshape.254), kind=kOutput, calls=%fused_computation.48 | convolution fusion | flops 100794368 | bytes 1314816 | tf_op jit(solution)/shard_map/nhkd,nhkv->nhdv/dot_general | solution.py:92
  47.3 28.8 %all-gather.9.cloned.1.call-done = bf16[576,2048]{1,0:T(8,128)(2,1)} async-done(((bf16[576,512]{1,0:T(8,128)(2,1)}), bf16[576,2048]{1,0:T(8,128)(2,1)}) %all-gather.9.cloned.1.call-update) | async-done | bytes 2359312 | tf_op jit(solution)/shard_map/all_gather | solution.py:211
  76.1 5.2 %fusion.5 = f32[576,1024]{1,0:T(8,128)S(1)} fusion(bf16[576,2048]{1,0:T(8,128)(2,1)} %all-gather.9.cloned.1.call-done, bf16[1,2048,1024]{2,1,0:T(8,128)(2,1)} %param.36), kind=kOutput, calls=%fused_computation.12 | convolution fusion | flops 2415919104 | bytes 8912896 | tf_op jit(solution)/shard_map/dot_general | solution.py:212
  81.3 3.9 %multiply_convert_fusion = bf16[576,1024]{1,0:T(8,128)(2,1)} fusion(f32[576,1024]{1,0:T(8,128)S(1)} %fusion.5, bf16[576,2048]{1,0:T(8,128)(2,1)S(1)} %copy-done.20, bf16[1,2048,1024]{2,1,0:T(8,128)(2,1)S(1)} %copy-done.19), kind=kOutput, calls=%fused_computation.14 | convolution fusion | flops 2419458048 | bytes 10092544 | tf_op jit(solution)/shard_map/dot_general | solution.py:213
  85.3 6.9 %while.27 = (s32[]{:T(128)}, f32[4,64,128]{2,1,0:T(8,128)S(1)}, f32[4,4,64,128]{3,2,1,0:T(8,128)}, f32[4,4,64]{2,1,0:T(4,128)S(1)}, f32[4,4,64,128]{3,2,1,0:T(8,128)}, /*index=5*/s32[]{:T(128)}, s32[]{:T(128)}) while((s32[]{:T(128)}, f32[4,64,128]{2,1,0:T(8,128)S(1)}, f32[4,4,64,128]{3,2,1,0:T(8,128)}, f32[4,4,64]{2,1,0:T(4,128)S(1)}, ...), condition=%wide.region_2.3_spmd.clone, body=%wide.region_1.2_spmd.clone.sunk | while | flops 131075 | bytes 659040 | solution.py:104
  92.8 2.0 reshape.266
  94.8 12.5 %all-gather.2 = bf16[8,4,64]{2,1,0:T(4,128)(2,1)} all-gather(bf16[1,4,64]{2,1,0:T(4,128)(2,1)S(1)} %fusion.52), channel_id=2, replica_groups=mesh['ep'=8,'tp'=4] {'ep'}, dimensions={0}, use_global_device_ids=true | all-gather | bytes 4608 | tf_op jit(solution)/shard_map/all_gather | solution.py:16
  107.3 16.2 %all-gather.1 = bf16[32,64,128]{2,1,0:T(8,128)(2,1)} all-gather(bf16[4,64,128]{2,1,0:T(8,128)(2,1)} %convert_element_type.87), channel_id=3, replica_groups=mesh['ep'=8,'tp'=4] {'ep'}, dimensions={0}, use_global_device_ids=true | all-gather | bytes 589824 | tf_op jit(solution)/shard_map/all_gather | solution.py:16
  123.6 2.1 %convolution_select_fusion = f32[4,4,64,64]{3,2,1,0:T(8,128)S(1)} fusion(f32[4,4,64,64]{3,2,1,0:T(8,128)S(1)} %reduce_window_sum.37, f32[4,64,4,64]{3,2,1,0:T(4,128)S(1)} %reshape.267, f32[4,64,4,64]{3,2,1,0:T(4,128)} %reshape.266, pred[64,64]{1,0:T(8,128)(4,1)S(1)} %iota_compare_fusion.1), kind=kOutput, calls=%fused_computation.16 | convolution fusion | flops 50593792 | bytes 1052672 | tf_op jit(solution)/shard_map/nhqd,nhkd->nhqk/dot_general | solution.py:87
  126.9 13.2 %while.28 = (s32[]{:T(128)}, f32[4,64,128]{2,1,0:T(8,128)S(1)}, s32[]{:T(128)}, bf16[8,4,64]{2,1,0:T(4,128)(2,1)}, bf16[8,4,64,128]{3,2,1,0:T(8,128)(2,1)}, /*index=5*/s32[]{:T(128)}, s32[]{:T(128)}) while((s32[]{:T(128)}, f32[4,64,128]{2,1,0:T(8,128)S(1)}, s32[]{:T(128)}, bf16[8,4,64]{2,1,0:T(4,128)(2,1)}, ...), condition=%wide.region_6.7_spmd.clone, body=%wide.region_5.6_spmd.clone.sunk | while | flops 164100 | bytes 330345 | solution.py:33
  140.1 2.8 %multiply_reduce_fusion.1 = (f32[4,64,4]{1,2,0:T(4,128)S(1)}, f32[4,64,4,128]{3,1,2,0:T(8,128)}) fusion(f32[4,4,64,128]{3,2,1,0:T(8,128)} %fusion.37, f32[4,4,64,128]{3,2,1,0:T(8,128)} %get-tuple-element.124, f32[4,64,128]{2,1,0:T(8,128)S(1)} %get-tuple-element.126, f32[4,4,64]{2,1,0:T(4,128)S(1)} %fusion.14, f32[4,64,4,64]{3,2,1,0:T(4,128)S(1)} %copy-done.2, ...), kind=kOutput, calls=%fused_computation.52 | convolution fusion | flops 101383168 | bytes 2236416 | tf_op jit(solution)/shard_map/nhqd,nhdv->nhqv/dot_general | solution.py:110
  144.8 1.6 fusion.31
  150.1 1.6 fusion.53
  151.6 2.2 %fusion.13 = bf16[96,256]{1,0:T(8,128)(2,1)} fusion(bf16[96,2048]{1,0:T(8,128)(2,1)S(1)} %copy-done.4, bf16[2048,256]{1,0:T(8,128)(2,1)} %param.40, f32[96,256]{1,0:T(8,128)S(1)} %fusion.53), kind=kOutput, calls=%fused_computation.21 | convolution fusion | flops 100810752 | bytes 1589248 | tf_op jit(solution)/shard_map/dot_general | solution.py:217
  154.6 8.7 %all_gather.28 = bf16[24,4096]{1,0:T(8,128)(2,1)S(1)} all-gather(bf16[24,1024]{1,0:T(8,128)(2,1)S(1)} %reshape.261), channel_id=1, replica_groups=mesh['ep'=8,'tp'=4] {'tp'}, dimensions={1}, use_global_device_ids=true | all-gather | bytes 245760 | tf_op jit(solution)/shard_map/all_gather | solution.py:228
  166.5 7.1 %fusion.9 = bf16[576,512]{1,0:T(8,128)(2,1)} fusion(bf16[576,4096]{1,0:T(8,128)(2,1)} %all-gather.11.cloned.1.call-done, bf16[1,4096,512]{2,1,0:T(8,128)(2,1)} %param.38), kind=kOutput, calls=%fused_computation.15 | convolution fusion | flops 2416214016 | bytes 9502720 | tf_op jit(solution)/shard_map/dot_general | solution.py:229
  173.6 3.7 %all-to-all-start.1 = ((bf16[8,72,512]{2,1,0:T(8,128)(2,1)}), bf16[8,72,512]{2,1,0:T(8,128)(2,1)S(1)}, u32[]{:S(2)}, u32[]{:S(2)}) async-start(bf16[8,72,512]{2,1,0:T(8,128)(2,1)} %bitcast.17), calls=%async_computation.1 | async-start | bytes 1179648 | tf_op jit(solution)/shard_map/all_to_all | solution.py:234
  182.5 2.6 %convolution_convert_fusion = bf16[256,512]{1,0:T(8,128)(2,1)} fusion(bf16[256,2048]{1,0:T(8,128)(2,1)} %all-gather.7.cloned.1.call-done, bf16[2048,512]{1,0:T(8,128)(2,1)S(1)} %copy-done), kind=kOutput, calls=%fused_computation.19 | convolution fusion | flops 537001984 | bytes 3407872 | tf_op jit(solution)/shard_map/dot_general | solution.py:222
  185.2 8.7 %all-to-all-done.1 = bf16[8,72,512]{2,1,0:T(8,128)(2,1)S(1)} async-done(((bf16[8,72,512]{2,1,0:T(8,128)(2,1)}), bf16[8,72,512]{2,1,0:T(8,128)(2,1)S(1)}, u32[]{:S(2)}, u32[]{:S(2)}) %all-to-all-start.1) | async-done | bytes 589856 | tf_op jit(solution)/shard_map/all_to_all | solution.py:234
  193.9 2.1 %gather_fusion.1 = bf16[384,512]{1,0:T(8,128)(2,1)S(1)} fusion(bf16[576,512]{1,0:T(8,128)(2,1)S(1)} %bitcast.126, s32[1024]{0:T(1024)S(1)} %pad_clamp_fusion), kind=kCustom, calls=%fused_computation.1 | custom fusion | bytes 787968 | tf_op jit(solution)/shard_map/jit(_take)/gather | solution.py:237
  (146 shorter events, 46.3 us)
Async XLA Ops:
  7.2 175.4 %copy-start = (bf16[2048,512]{1,0:T(8,128)(2,1)S(1)}, bf16[2048,512]{1,0:T(8,128)(2,1)}, u32[]{:S(2)}) copy-start(bf16[2048,512]{1,0:T(8,128)(2,1)} %param.31) | copy-start | bytes 6291460
  7.2 68.9 %all-gather.9.cloned.1.call-start = ((), (), s32[]{:S(2)}) async-start(), calls=%async_computation.3 | async-start | bytes 2949120 | tf_op jit(solution)/shard_map/all_gather | solution.py:211
  12.9 0.8 copy-start.3
  16.5 23.4 %copy-start.11 = (bf16[256,256]{1,0:T(8,128)(2,1)S(1)}, bf16[256,256]{1,0:T(8,128)(2,1)}, u32[]{:S(2)}) copy-start(bf16[256,256]{1,0:T(8,128)(2,1)} %param.27) | copy-start | bytes 393220
  16.5 23.4 %copy-start.18 = (f32[256]{0:T(256)S(1)}, f32[256]{0:T(256)}, u32[]{:S(2)}) copy-start(f32[256]{0:T(256)} %param.28) | copy-start | bytes 3076
  16.5 23.8 %copy-start.16 = (f32[4,256]{1,0:T(4,128)S(1)}, f32[4,256]{1,0:T(4,128)}, u32[]{:S(2)}) copy-start(f32[4,256]{1,0:T(4,128)} %param.29) | copy-start | bytes 12292
  16.5 23.9 %copy-start.12 = (bf16[256,256]{1,0:T(8,128)(2,1)S(1)}, bf16[256,256]{1,0:T(8,128)(2,1)}, u32[]{:S(2)}) copy-start(bf16[256,256]{1,0:T(8,128)(2,1)} %param.24) | copy-start | bytes 393220
  39.8 126.7 %all-gather.11.cloned.1.call-start = ((), (), s32[]{:S(2)}) async-start(), calls=%async_computation.4 | async-start | bytes 5898240 | tf_op jit(solution)/shard_map/all_gather | solution.py:227
  76.1 5.2 %copy-start.19 = (bf16[1,2048,1024]{2,1,0:T(8,128)(2,1)S(1)}, bf16[1,2048,1024]{2,1,0:T(8,128)(2,1)}, u32[]{:S(2)}) copy-start(bf16[1,2048,1024]{2,1,0:T(8,128)(2,1)} %param.37) | copy-start | bytes 12582916
  76.1 5.3 %copy-start.20 = (bf16[576,2048]{1,0:T(8,128)(2,1)S(1)}, bf16[576,2048]{1,0:T(8,128)(2,1)}, u32[]{:S(2)}) copy-start(bf16[576,2048]{1,0:T(8,128)(2,1)} %all-gather.9.cloned.1.call-done) | copy-start | bytes 7077892
  85.2 97.3 %all-gather.7.cloned.1.call-start = ((), (), s32[]{:S(2)}) async-start(), calls=%async_computation.2 | async-start | bytes 1310720 | tf_op jit(solution)/shard_map/all_gather | solution.py:223
  92.8 32.9 %copy-start.5 = (bf16[4,64,4,128]{3,2,1,0:T(4,128)(2,1)S(1)}, bf16[4,64,4,128]{3,2,1,0:T(4,128)(2,1)}, u32[]{:S(2)}) copy-start(bf16[4,64,4,128]{3,2,1,0:T(4,128)(2,1)} %reshape.254) | copy-start | bytes 786436
  125.7 14.4 %copy-start.2 = (f32[4,64,4,64]{3,2,1,0:T(4,128)S(1)}, f32[4,64,4,64]{3,2,1,0:T(4,128)}, u32[]{:S(2)}) copy-start(f32[4,64,4,64]{3,2,1,0:T(4,128)} %reshape.266) | copy-start | bytes 786436
  140.1 4.7 %copy-start.6 = (bf16[256,512]{1,0:T(8,128)(2,1)S(1)}, bf16[256,512]{1,0:T(8,128)(2,1)}, u32[]{:S(2)}) copy-start(bf16[256,512]{1,0:T(8,128)(2,1)} %param.26) | copy-start | bytes 786436
  142.9 3.5 %copy-start.15 = (s32[96,4]{0,1:T(4,128)S(1)}, s32[96,4]{0,1:T(4,128)}, u32[]{:S(2)}) copy-start(s32[96,4]{0,1:T(4,128)} %param.34) | copy-start | bytes 4612
  142.9 3.5 %copy-start.14 = (s32[384]{0:T(512)S(1)}, s32[384]{0:T(512)}, u32[]{:S(2)}) copy-start(s32[384]{0:T(512)} %copy-done.13) | copy-start | bytes 4612
  142.9 7.1 %copy-start.4 = (bf16[96,2048]{1,0:T(8,128)(2,1)S(1)}, bf16[96,2048]{1,0:T(8,128)(2,1)}, u32[]{:S(2)}) copy-start(bf16[96,2048]{1,0:T(8,128)(2,1)} %copy-done.3) | copy-start | bytes 1179652
  147.2 18.5 %copy-start.1 = (bf16[1024,512]{1,0:T(8,128)(2,1)S(1)}, bf16[1024,512]{1,0:T(8,128)(2,1)}, u32[]{:S(2)}) copy-start(bf16[1024,512]{1,0:T(8,128)(2,1)} %param.41) | copy-start | bytes 3145732
  166.5 10.8 %copy-start.8 = (bf16[3,8,4,256]{3,1,2,0:T(8,128)(2,1)S(1)}, bf16[3,8,4,256]{3,1,2,0:T(8,128)(2,1)}, u32[]{:S(2)}) copy-start(bf16[3,8,4,256]{3,1,2,0:T(8,128)(2,1)} %copy.114) | copy-start | bytes 147460
  173.6 5.4 %copy-start.17 = (pred[96,4]{0,1:T(4,128)(4,1)S(1)}, pred[96,4]{0,1:T(4,128)(4,1)}, u32[]{:S(2)}) copy-start(pred[96,4]{0,1:T(4,128)(4,1)} %compare_and_fusion) | copy-start | bytes 1156
  173.6 5.6 %copy-start.10 = (bf16[24,4,256]{2,1,0:T(4,128)(2,1)S(1)}, bf16[24,4,256]{2,1,0:T(4,128)(2,1)}, u32[]{:S(2)}) copy-start(bf16[24,4,256]{2,1,0:T(4,128)(2,1)} %get-tuple-element.166) | copy-start | bytes 147460
  173.6 5.7 %copy-start.9 = (bf16[24,4,256]{2,1,0:T(4,128)(2,1)S(1)}, bf16[24,4,256]{2,1,0:T(4,128)(2,1)}, u32[]{:S(2)}) copy-start(bf16[24,4,256]{2,1,0:T(4,128)(2,1)} %get-tuple-element.163) | copy-start | bytes 147460
  173.6 8.6 %copy-start.7 = (f32[24,1,512]{2,0,1:T(8,128)S(1)}, f32[24,1,512]{2,0,1:T(8,128)}, u32[]{:S(2)}) copy-start(f32[24,1,512]{2,0,1:T(8,128)} %convolution_bitcast_fusion) | copy-start | bytes 147460
  173.6 20.3 %all-to-all-start.1 = ((bf16[8,72,512]{2,1,0:T(8,128)(2,1)}), bf16[8,72,512]{2,1,0:T(8,128)(2,1)S(1)}, u32[]{:S(2)}, u32[]{:S(2)}) async-start(bf16[8,72,512]{2,1,0:T(8,128)(2,1)} %bitcast.17), calls=%async_computation.1 | async-start | bytes 1179648 | tf_op jit(solution)/shard_map/all_to_all | solution.py:234
  (1 other events, 0.6 us)
Sparse Core Ops, SparseCore 0:
  39.9 36.1 all-gather.8
  85.4 56.9 all-gather.10
  146.5 25.0 all-gather.6
where the time goes:
time: 206 us; the launch traced here: 204 us
  blocking collectives  60.4 us (29%)
  waiting for transfers between devices  37.6 us (18%)
  matrix products  36.3 us (18%)
  other arithmetic  31.8 us (15%)
  local copies, waits for them, and re-layouts  19.5 us (9%)
  between operations  14.3 us (7%)
  starting transfers between devices  3.8 us (2%)
    all_gather x1, waiting for transfers between devices, local(): section = lax.all_gather(flat_columns, 'tp', axis=1, tiled=True)  28.8 us
    all_gather x2, blocking collectives, entering(): lax.all_gather(part.astype(kind), axis)  28.7 us
    all_to_all x1, blocking collectives, local(): lax.all_to_all(outgoing, 'ep', split_axis=0, concat_axis=0, tiled=True)  23 us
    all_to_all x1, waiting for transfers between devices, local(): lax.all_to_all(routed_output, 'ep', split_axis=0, concat_axis=0, tiled=True)  8.75 us
    all_gather x1, blocking collectives, local(): shared_section = lax.all_gather(shared_paired, 'tp', axis=1, tiled=True)  8.68 us
    select_n x8, other arithmetic, hop(): return jax.tree.map(lambda a, b: jnp.where(reached, a, b), new, before)  7.73 us
    dot_general x1, matrix products, local(): jnp.dot(routed_section, down_weight, preferred_element_type=jnp.float32)  7.07 us
    dot_general x4, matrix products, paired_product(): jnp.dot(pieces[:, :, which, :].reshape(row_count, -1), weight, preferred_...  5.29 us
  transfers between devices with their start and end apart: 4, of which 2 were waited for; matrix products, arithmetic and copies ran while one was open for 32% of the time, Pallas kernels for 0%

commit v1 on v0

--- a/solution.py
+++ b/solution.py
@@ -8,6 +8,24 @@
 temper = 16.0
 routed_scale = 2.5
 largest_value = lax.Precision.HIGHEST
+
+
+def guide_bench(my_data, k_dim, here_x):
+    tmp, mat_out = (my_data.shape[:k_dim], my_data.shape[k_dim + 1 :])
+    s_next = my_data.reshape(*tmp, here_x, -1, *mat_out)
+    x_new = jnp.moveaxis(s_next, k_dim, 0)
+    return x_new
+
+
+def _close_ends(local_block, where_dim):
+    local_block = jnp.moveaxis(local_block, 0, where_dim)
+    block_out = local_block.shape
+    big = local_block.reshape(
+        *block_out[:where_dim],
+        block_out[where_dim] * block_out[where_dim + 1],
+        *block_out[where_dim + 2 :]
+    )
+    return big
 
 
 def entering(value, axis, combine, identity):
@@ -180,6 +198,24 @@
     shared_up_weight,
     shared_down_weight,
 ):
+
+    def show_widths_in(local_x, axis_tag, z_in, view):
+        known = lax.axis_size(axis_tag)
+        a_now = lax.axis_index(axis_tag)
+        upper, state_next = (known, a_now)
+        r2 = guide_bench(local_x, z_in, upper)
+        r_now = r2
+        for it in range(1, upper):
+            y1, u_next = ((state_next + it) % upper, (state_next - it) % upper)
+            arr_out = lax.dynamic_index_in_dim(r2, y1, 0)
+            val2 = range(upper)
+            kept_arr = map(lambda i0: (i0, (i0 + it) % upper), val2)
+            u1 = list(kept_arr)
+            prior = lax.ppermute(arr_out, axis_tag, u1)
+            r_now = lax.dynamic_update_slice_in_dim(r_now, prior, u_next, axis=0)
+        outer = _close_ends(r_now, view)
+        return outer
+
     mixed_heads = mixer_heads(
         first_batch_queries,
         first_batch_keys,
@@ -231,9 +267,7 @@
     shared_total = shared_part.reshape(tokens, -1)
     token_mixed = mixer_total.astype(jnp.bfloat16)
     routed_output = routed_part.astype(jnp.bfloat16).reshape(experts, capacity, -1)
-    returned = lax.all_to_all(routed_output, "ep", split_axis=0, concat_axis=0, tiled=True).reshape(
-        slot_count, -1
-    )
+    returned = show_widths_in(routed_output, "ep", 0, 0).reshape(slot_count, -1)
     picked = jnp.take(returned, slot_ids, axis=0).astype(jnp.float32).reshape(tokens, top_count, -1)
     weights = (
         routed_scale * router_chosen_scores / jnp.sum(router_chosen_scores, axis=1, keepdims=True)

time: 206 us -> 198 us (0.961)
  other arithmetic: 31.8 us -> 26.3 us
  matrix products: 36.3 us -> 31.3 us
  starting transfers between devices: 3.8 us -> 6.94 us
    all_to_all x1 -> x0, waiting for transfers between devices: 8.75 us -> none  [local(): lax.all_to_all(routed_output, 'ep', split_axis=0, concat_axis=0, tiled=True)]
    ppermute x0 -> x7, waiting for transfers between devices: none -> 8.4 us  [show_widths_in(): prior = lax.ppermute(arr_out, axis_tag, u1)]
    ppermute x0 -> x7, starting transfers between devices: none -> 6.82 us  [show_widths_in(): prior = lax.ppermute(arr_out, axis_tag, u1)]
    convert_element_type x8, other arithmetic: 5.27 us -> 0.06 us  [hop(): part[k].astype(own.dtype)]
    dot_general x4, matrix products: 5.29 us -> 0.98 us  [paired_product(): jnp.dot(pieces[:, :, which, :].reshape(row_count, -1), weight, preferred_...]
    all_to_all x1 -> x0, starting transfers between devices: 3.68 us -> none  [local(): lax.all_to_all(routed_output, 'ep', split_axis=0, concat_axis=0, tiled=True)]
  transfers between devices with their start and end apart: 4 -> 10, of which waited for: 2 -> 5; matrix products, arithmetic and copies ran while one was open for 32% -> 28% of each run, Pallas kernels for 0% -> 0%
where the time goes in v1:
time: 198 us; the launch traced here: 195 us
  blocking collectives  60.6 us (31%)
  waiting for transfers between devices  37.3 us (19%)
  matrix products  31.3 us (16%)
  other arithmetic  26.3 us (13%)
  local copies, waits for them, and re-layouts  17.7 us (9%)
  between operations  14.5 us (7%)
  starting transfers between devices  6.94 us (4%)
    all_gather x1, waiting for transfers between devices, local(): section = lax.all_gather(flat_columns, 'tp', axis=1, tiled=True)  28.8 us
    all_gather x2, blocking collectives, entering(): lax.all_gather(part.astype(kind), axis)  27.9 us
    all_to_all x1, blocking collectives, local(): lax.all_to_all(outgoing, 'ep', split_axis=0, concat_axis=0, tiled=True)  23 us
    all_gather x1, blocking collectives, local(): shared_section = lax.all_gather(shared_paired, 'tp', axis=1, tiled=True)  9.74 us
    ppermute x7, waiting for transfers between devices, show_widths_in(): prior = lax.ppermute(arr_out, axis_tag, u1)  8.4 us
    select_n x8, other arithmetic, hop(): return jax.tree.map(lambda a, b: jnp.where(reached, a, b), new, before)  7.76 us
    ppermute x7, starting transfers between devices, show_widths_in(): prior = lax.ppermute(arr_out, axis_tag, u1)  6.82 us
    dot_general x1, matrix products, local(): jnp.dot(routed_section, down_weight, preferred_element_type=jnp.float32)  6.39 us
  transfers between devices with their start and end apart: 10, of which 5 were waited for; matrix products, arithmetic and copies ran while one was open for 28% of the time, Pallas kernels for 0%

profile of v1, /device:TPU:0, one launch (start us, length us, event | category | flops | bytes accessed | tf_op | source)
XLA Modules:
  0.0 195.0 jit_solution(16255703731687574404)
XLA Ops:
  13.1 2.7 %gather_fusion = bf16[576,512]{1,0:T(8,128)(2,1)S(1)} fusion(bf16[96,512]{1,0:T(8,128)(2,1)S(1)} %constant_dynamic-slice_fusion.7, s32[1024]{0:T(1024)S(1)} %pad_clamp_fusion.1), kind=kCustom, calls=%fused_computation | custom fusion | bytes 1181952 | tf_op jit(solution)/shard_map/jit(_take)/gather | solution.py:158
  16.2 23.0 %all_to_all.5 = bf16[8,72,512]{2,1,0:T(8,128)(2,1)} all-to-all(bf16[8,72,512]{2,1,0:T(8,128)(2,1)S(1)} %select_select_fusion), channel_id=1, replica_groups=mesh['ep'=8,'tp'=4] {'ep'}, dimensions={0} | all-to-all | bytes 1179648 | tf_op jit(solution)/shard_map/all_to_all | solution.py:245
  40.1 1.7 reshape.248
  44.3 2.4 %fusion.23 = f32[4,4,64,128]{3,2,1,0:T(8,128)} fusion(f32[4,4,64,64]{3,2,1,0:T(8,128)S(1)} %reduce_window_sum.37, f32[4,64,4,64]{3,2,1,0:T(4,128)S(1)} %reshape.259, f32[4,4,64]{2,1,0:T(4,128)S(1)} %bitcast.135, bf16[4,64,4,128]{3,2,1,0:T(4,128)(2,1)} %reshape.248), kind=kOutput, calls=%fused_computation.48 | convolution fusion | flops 100794368 | bytes 1314816 | tf_op jit(solution)/shard_map/nhkd,nhkv->nhdv/dot_general | solution.py:110
  46.7 28.8 %all-gather.9.cloned.1.call-done = bf16[576,2048]{1,0:T(8,128)(2,1)} async-done(((bf16[576,512]{1,0:T(8,128)(2,1)}), bf16[576,2048]{1,0:T(8,128)(2,1)}) %all-gather.9.cloned.1.call-update) | async-done | bytes 2359312 | tf_op jit(solution)/shard_map/all_gather | solution.py:247
  75.5 5.2 %fusion.5 = f32[576,1024]{1,0:T(8,128)S(1)} fusion(bf16[576,2048]{1,0:T(8,128)(2,1)} %all-gather.9.cloned.1.call-done, bf16[1,2048,1024]{2,1,0:T(8,128)(2,1)} %param.36), kind=kOutput, calls=%fused_computation.12 | convolution fusion | flops 2415919104 | bytes 8912896 | tf_op jit(solution)/shard_map/dot_general | solution.py:248
  80.8 3.9 %multiply_convert_fusion = bf16[576,1024]{1,0:T(8,128)(2,1)} fusion(f32[576,1024]{1,0:T(8,128)S(1)} %fusion.5, bf16[576,2048]{1,0:T(8,128)(2,1)S(1)} %copy-done.14, bf16[1,2048,1024]{2,1,0:T(8,128)(2,1)S(1)} %copy-done.13), kind=kOutput, calls=%fused_computation.14 | convolution fusion | flops 2419458048 | bytes 10092544 | tf_op jit(solution)/shard_map/dot_general | solution.py:249
  84.7 6.9 %while.27 = (s32[]{:T(128)}, f32[4,64,128]{2,1,0:T(8,128)S(1)}, f32[4,4,64,128]{3,2,1,0:T(8,128)}, f32[4,4,64]{2,1,0:T(4,128)S(1)}, f32[4,4,64,128]{3,2,1,0:T(8,128)}, /*index=5*/s32[]{:T(128)}, s32[]{:T(128)}) while((s32[]{:T(128)}, f32[4,64,128]{2,1,0:T(8,128)S(1)}, f32[4,4,64,128]{3,2,1,0:T(8,128)}, f32[4,4,64]{2,1,0:T(4,128)S(1)}, ...), condition=%wide.region_2.3_spmd.clone, body=%wide.region_1.2_spmd.clone.sunk | while | flops 131075 | bytes 659040 | solution.py:122
  91.6 2.0 %reshape.258 = f32[4,64,4,64]{3,2,1,0:T(4,128)} reshape(bf16[256,256]{1,0:T(8,128)(2,1)} %param.23) | data formatting | bytes 393216 | tf_op jit(solution)/shard_map/transpose | solution.py:91
  93.6 11.8 %all-gather.2 = bf16[8,4,64]{2,1,0:T(4,128)(2,1)S(1)} all-gather(bf16[1,4,64]{2,1,0:T(4,128)(2,1)S(1)} %fusion.52), channel_id=2, replica_groups=mesh['ep'=8,'tp'=4] {'ep'}, dimensions={0}, use_global_device_ids=true | all-gather | bytes 4608 | tf_op jit(solution)/shard_map/all_gather | solution.py:34
  105.5 16.0 %all-gather.1 = bf16[32,64,128]{2,1,0:T(8,128)(2,1)} all-gather(bf16[4,64,128]{2,1,0:T(8,128)(2,1)S(1)} %convert_element_type.87), channel_id=3, replica_groups=mesh['ep'=8,'tp'=4] {'ep'}, dimensions={0}, use_global_device_ids=true | all-gather | bytes 589824 | tf_op jit(solution)/shard_map/all_gather | solution.py:34
  121.5 2.1 %convolution_select_fusion = f32[4,4,64,64]{3,2,1,0:T(8,128)S(1)} fusion(f32[4,4,64,64]{3,2,1,0:T(8,128)S(1)} %reduce_window_sum.37, f32[4,64,4,64]{3,2,1,0:T(4,128)S(1)} %reshape.259, f32[4,64,4,64]{3,2,1,0:T(4,128)} %reshape.258, pred[64,64]{1,0:T(8,128)(4,1)S(1)} %iota_compare_fusion.1), kind=kOutput, calls=%fused_computation.16 | convolution fusion | flops 50593792 | bytes 1052672 | tf_op jit(solution)/shard_map/nhqd,nhkd->nhqk/dot_general | solution.py:105
  124.9 8.1 %while.28 = (s32[]{:T(128)}, f32[4,64,128]{2,1,0:T(8,128)S(1)}, s32[]{:T(128)}, bf16[8,4,64]{2,1,0:T(4,128)(2,1)S(1)}, bf16[8,4,64,128]{3,2,1,0:T(8,128)(2,1)}, /*index=5*/s32[]{:T(128)}, s32[]{:T(128)}) while((s32[]{:T(128)}, f32[4,64,128]{2,1,0:T(8,128)S(1)}, s32[]{:T(128)}, bf16[8,4,64]{2,1,0:T(4,128)(2,1)S(1)}, ...), condition=%wide.region_6.7_spmd.clone, body=%wide.region_5.6_spmd.clone.sunk | while | flops 164100 | bytes 330345 | solution.py:51
  133.0 2.8 %multiply_reduce_fusion.1 = (f32[4,64,4]{1,2,0:T(4,128)S(1)}, f32[4,64,4,128]{3,1,2,0:T(8,128)}) fusion(f32[4,4,64,128]{3,2,1,0:T(8,128)} %fusion.37, f32[4,4,64,128]{3,2,1,0:T(8,128)} %get-tuple-element.124, f32[4,64,128]{2,1,0:T(8,128)S(1)} %get-tuple-element.126, f32[4,4,64]{2,1,0:T(4,128)S(1)} %fusion.14, f32[4,64,4,64]{3,2,1,0:T(4,128)S(1)} %copy-done.2, ...), kind=kOutput, calls=%fused_computation.52 | convolution fusion | flops 101383168 | bytes 2236416 | tf_op jit(solution)/shard_map/nhqd,nhdv->nhqv/dot_general | solution.py:128
  137.6 1.8 fusion.31
  144.7 2.2 %fusion.13 = bf16[96,256]{1,0:T(8,128)(2,1)} fusion(bf16[96,2048]{1,0:T(8,128)(2,1)S(1)} %copy-done.4, bf16[2048,256]{1,0:T(8,128)(2,1)} %param.40, f32[96,256]{1,0:T(8,128)S(1)} %fusion.53), kind=kOutput, calls=%fused_computation.21 | convolution fusion | flops 100810752 | bytes 1589248 | tf_op jit(solution)/shard_map/dot_general | solution.py:253
  147.7 9.7 %all_gather.28 = bf16[24,4096]{1,0:T(8,128)(2,1)S(1)} all-gather(bf16[24,1024]{1,0:T(8,128)(2,1)S(1)} %reshape.253), channel_id=1, replica_groups=mesh['ep'=8,'tp'=4] {'tp'}, dimensions={1}, use_global_device_ids=true | all-gather | bytes 245760 | tf_op jit(solution)/shard_map/all_gather | solution.py:264
  160.5 6.4 %fusion.9 = bf16[576,512]{1,0:T(8,128)(2,1)S(1)} fusion(bf16[576,4096]{1,0:T(8,128)(2,1)} %all-gather.11.cloned.1.call-done, bf16[1,4096,512]{2,1,0:T(8,128)(2,1)} %param.38), kind=kOutput, calls=%fused_computation.15 | convolution fusion | flops 2416214016 | bytes 9502720 | tf_op jit(solution)/shard_map/dot_general | solution.py:265
  167.0 5.5 %collective-permute-done = bf16[1,1,72,512]{3,2,0,1:T(8,128)(2,1)S(1)} collective-permute-done((bf16[1,1,72,512]{3,2,0,1:T(8,128)(2,1)S(1)}, bf16[1,1,72,512]{3,2,0,1:T(8,128)(2,1)S(1)}, u32[]{:S(2)}, u32[]{:S(2)}) %collective-permute-start) | collective-permute-done | bytes 73760 | tf_op jit(solution)/shard_map/ppermute | solution.py:214
  172.7 2.6 %convolution_convert_fusion = bf16[256,512]{1,0:T(8,128)(2,1)} fusion(bf16[256,2048]{1,0:T(8,128)(2,1)} %all-gather.7.cloned.1.call-done, bf16[2048,512]{1,0:T(8,128)(2,1)S(1)} %copy-done), kind=kOutput, calls=%fused_computation.19 | convolution fusion | flops 537001984 | bytes 3407872 | tf_op jit(solution)/shard_map/dot_general | solution.py:258
  176.4 1.6 collective-permute-start.4
  178.0 3.8 %collective-permute-start.5 = (bf16[1,1,72,512]{3,2,0,1:T(8,128)(2,1)S(1)}, bf16[1,1,72,512]{3,2,0,1:T(8,128)(2,1)S(1)}, u32[]{:S(2)}, u32[]{:S(2)}) collective-permute-start(bf16[1,1,72,512]{3,2,0,1:T(8,128)(2,1)S(1)} %get-tuple-element.188), channel_id=1, source_target_pairs={{0,24},{4,28},{8,0},{12,4},{16,8},{20,12},{24,16},{28,20},{1,25},{... | collective-permute-start | bytes 221192 | tf_op jit(solution)/shard_map/ppermute | solution.py:214
  182.6 1.6 collective-permute-done.3
  185.0 2.1 %gather_fusion.1 = bf16[384,512]{1,0:T(8,128)(2,1)S(1)} fusion(bf16[576,512]{1,0:T(8,128)(2,1)S(1)} %bitcast.128, s32[1024]{0:T(1024)S(1)} %pad_clamp_fusion), kind=kCustom, calls=%fused_computation.1 | custom fusion | bytes 787968 | tf_op jit(solution)/shard_map/jit(_take)/gather | solution.py:271
  (154 shorter events, 40.3 us)
Async XLA Ops:
  7.2 165.5 %copy-start = (bf16[2048,512]{1,0:T(8,128)(2,1)S(1)}, bf16[2048,512]{1,0:T(8,128)(2,1)}, u32[]{:S(2)}) copy-start(bf16[2048,512]{1,0:T(8,128)(2,1)} %param.31) | copy-start | bytes 6291460
  7.2 68.3 %all-gather.9.cloned.1.call-start = ((), (), s32[]{:S(2)}) async-start(), calls=%async_computation.2 | async-start | bytes 2949120 | tf_op jit(solution)/shard_map/all_gather | solution.py:247
  15.9 23.4 %copy-start.6 = (bf16[256,256]{1,0:T(8,128)(2,1)S(1)}, bf16[256,256]{1,0:T(8,128)(2,1)}, u32[]{:S(2)}) copy-start(bf16[256,256]{1,0:T(8,128)(2,1)} %param.27) | copy-start | bytes 393220
  15.9 23.4 %copy-start.12 = (f32[256]{0:T(256)S(1)}, f32[256]{0:T(256)}, u32[]{:S(2)}) copy-start(f32[256]{0:T(256)} %param.28) | copy-start | bytes 3076
  15.9 23.8 %copy-start.9 = (f32[4,256]{1,0:T(4,128)S(1)}, f32[4,256]{1,0:T(4,128)}, u32[]{:S(2)}) copy-start(f32[4,256]{1,0:T(4,128)} %param.29) | copy-start | bytes 12292
  15.9 23.9 %copy-start.7 = (bf16[256,256]{1,0:T(8,128)(2,1)S(1)}, bf16[256,256]{1,0:T(8,128)(2,1)}, u32[]{:S(2)}) copy-start(bf16[256,256]{1,0:T(8,128)(2,1)} %param.24) | copy-start | bytes 393220
  39.2 121.3 %all-gather.11.cloned.1.call-start = ((), (), s32[]{:S(2)}) async-start(), calls=%async_computation.3 | async-start | bytes 5898240 | tf_op jit(solution)/shard_map/all_gather | solution.py:263
  75.5 5.2 %copy-start.13 = (bf16[1,2048,1024]{2,1,0:T(8,128)(2,1)S(1)}, bf16[1,2048,1024]{2,1,0:T(8,128)(2,1)}, u32[]{:S(2)}) copy-start(bf16[1,2048,1024]{2,1,0:T(8,128)(2,1)} %param.37) | copy-start | bytes 12582916
  75.5 5.3 %copy-start.14 = (bf16[576,2048]{1,0:T(8,128)(2,1)S(1)}, bf16[576,2048]{1,0:T(8,128)(2,1)}, u32[]{:S(2)}) copy-start(bf16[576,2048]{1,0:T(8,128)(2,1)} %all-gather.9.cloned.1.call-done) | copy-start | bytes 7077892
  84.7 88.0 %all-gather.7.cloned.1.call-start = ((), (), s32[]{:S(2)}) async-start(), calls=%async_computation.1 | async-start | bytes 1310720 | tf_op jit(solution)/shard_map/all_gather | solution.py:259
  93.6 30.1 %copy-start.5 = (bf16[4,64,4,128]{3,2,1,0:T(4,128)(2,1)S(1)}, bf16[4,64,4,128]{3,2,1,0:T(4,128)(2,1)}, u32[]{:S(2)}) copy-start(bf16[4,64,4,128]{3,2,1,0:T(4,128)(2,1)} %reshape.248) | copy-start | bytes 786436
  123.7 9.3 %copy-start.2 = (f32[4,64,4,64]{3,2,1,0:T(4,128)S(1)}, f32[4,64,4,64]{3,2,1,0:T(4,128)}, u32[]{:S(2)}) copy-start(f32[4,64,4,64]{3,2,1,0:T(4,128)} %reshape.258) | copy-start | bytes 786436
  133.0 4.6 %copy-start.10 = (f32[512]{0:T(512)S(1)}, f32[512]{0:T(512)}, u32[]{:S(2)}) copy-start(f32[512]{0:T(512)} %param.30) | copy-start | bytes 6148
  135.8 3.7 %copy-start.8 = (s32[96,4]{0,1:T(4,128)S(1)}, s32[96,4]{0,1:T(4,128)}, u32[]{:S(2)}) copy-start(s32[96,4]{0,1:T(4,128)} %param.34) | copy-start | bytes 4612
  135.8 7.4 %copy-start.4 = (bf16[96,2048]{1,0:T(8,128)(2,1)S(1)}, bf16[96,2048]{1,0:T(8,128)(2,1)}, u32[]{:S(2)}) copy-start(bf16[96,2048]{1,0:T(8,128)(2,1)} %copy-done.3) | copy-start | bytes 1179652
  140.3 18.3 %copy-start.1 = (bf16[1024,512]{1,0:T(8,128)(2,1)S(1)}, bf16[1024,512]{1,0:T(8,128)(2,1)}, u32[]{:S(2)}) copy-start(bf16[1024,512]{1,0:T(8,128)(2,1)} %param.41) | copy-start | bytes 3145732
  157.6 2.1 %copy-start.11 = (pred[96,4]{0,1:T(4,128)(4,1)S(1)}, pred[96,4]{0,1:T(4,128)(4,1)}, u32[]{:S(2)}) copy-start(pred[96,4]{0,1:T(4,128)(4,1)} %compare_and_fusion) | copy-start | bytes 1156
  166.9 5.6 %collective-permute-start = (bf16[1,1,72,512]{3,2,0,1:T(8,128)(2,1)S(1)}, bf16[1,1,72,512]{3,2,0,1:T(8,128)(2,1)S(1)}, u32[]{:S(2)}, u32[]{:S(2)}) collective-permute-start(bf16[1,1,72,512]{3,2,0,1:T(8,128)(2,1)S(1)} %constant_dynamic-slice_fusion.6), channel_id=1, source_target_pairs={{0,4},{4,8},{8,12},{12,16},{16,20},{20,24},{24,28},{28,0},{1,5},{5... | collective-permute-start | bytes 221192 | tf_op jit(solution)/shard_map/ppermute | solution.py:214
  172.6 9.2 %collective-permute-start.1 = (bf16[1,1,72,512]{3,2,0,1:T(8,128)(2,1)S(1)}, bf16[1,1,72,512]{3,2,0,1:T(8,128)(2,1)S(1)}, u32[]{:S(2)}, u32[]{:S(2)}) collective-permute-start(bf16[1,1,72,512]{3,2,0,1:T(8,128)(2,1)S(1)} %get-tuple-element.192), channel_id=1, source_target_pairs={{0,8},{4,12},{8,16},{12,20},{16,24},{20,28},{24,0},{28,4},{1,9},{5... | collective-permute-start | bytes 221192 | tf_op jit(solution)/shard_map/ppermute | solution.py:214
  175.4 7.2 %collective-permute-start.2 = (bf16[1,1,72,512]{3,2,0,1:T(8,128)(2,1)S(1)}, bf16[1,1,72,512]{3,2,0,1:T(8,128)(2,1)S(1)}, u32[]{:S(2)}, u32[]{:S(2)}) collective-permute-start(bf16[1,1,72,512]{3,2,0,1:T(8,128)(2,1)S(1)} %get-tuple-element.191), channel_id=1, source_target_pairs={{0,12},{4,16},{8,20},{12,24},{16,28},{20,0},{24,4},{28,8},{1,13},{... | collective-permute-start | bytes 221192 | tf_op jit(solution)/shard_map/ppermute | solution.py:214
  175.4 8.9 %collective-permute-start.3 = (bf16[1,1,72,512]{3,2,0,1:T(8,128)(2,1)S(1)}, bf16[1,1,72,512]{3,2,0,1:T(8,128)(2,1)S(1)}, u32[]{:S(2)}, u32[]{:S(2)}) collective-permute-start(bf16[1,1,72,512]{3,2,0,1:T(8,128)(2,1)S(1)} %get-tuple-element.190), channel_id=1, source_target_pairs={{0,16},{4,20},{8,24},{12,28},{16,0},{20,4},{24,8},{28,12},{1,17},{... | collective-permute-start | bytes 221192 | tf_op jit(solution)/shard_map/ppermute | solution.py:214
  176.4 7.9 %collective-permute-start.4 = (bf16[1,1,72,512]{3,2,0,1:T(8,128)(2,1)S(1)}, bf16[1,1,72,512]{3,2,0,1:T(8,128)(2,1)S(1)}, u32[]{:S(2)}, u32[]{:S(2)}) collective-permute-start(bf16[1,1,72,512]{3,2,0,1:T(8,128)(2,1)S(1)} %get-tuple-element.189), channel_id=1, source_target_pairs={{0,20},{4,24},{8,28},{12,0},{16,4},{20,8},{24,12},{28,16},{1,21},{... | collective-permute-start | bytes 221192 | tf_op jit(solution)/shard_map/ppermute | solution.py:214
  178.0 7.0 %collective-permute-start.5 = (bf16[1,1,72,512]{3,2,0,1:T(8,128)(2,1)S(1)}, bf16[1,1,72,512]{3,2,0,1:T(8,128)(2,1)S(1)}, u32[]{:S(2)}, u32[]{:S(2)}) collective-permute-start(bf16[1,1,72,512]{3,2,0,1:T(8,128)(2,1)S(1)} %get-tuple-element.188), channel_id=1, source_target_pairs={{0,24},{4,28},{8,0},{12,4},{16,8},{20,12},{24,16},{28,20},{1,25},{... | collective-permute-start | bytes 221192 | tf_op jit(solution)/shard_map/ppermute | solution.py:214
  181.8 3.2 %collective-permute-start.6 = (bf16[1,1,72,512]{3,2,0,1:T(8,128)(2,1)S(1)}, bf16[1,1,72,512]{3,2,0,1:T(8,128)(2,1)S(1)}, u32[]{:S(2)}, u32[]{:S(2)}) collective-permute-start(bf16[1,1,72,512]{3,2,0,1:T(8,128)(2,1)S(1)} %get-tuple-element.187), channel_id=1, source_target_pairs={{0,28},{4,0},{8,4},{12,8},{16,12},{20,16},{24,20},{28,24},{1,29},{... | collective-permute-start | bytes 221192 | tf_op jit(solution)/shard_map/ppermute | solution.py:214
  (1 other events, 0.8 us)
Sparse Core Ops, SparseCore 0:
  39.3 36.1 all-gather.8
  84.8 56.9 all-gather.10
  144.2 26.3 all-gather.6
